TPU v7x, 32 devices: a whole 2x2x4 slice. The times are simulated.
32 devices in a mesh: sp: 16 (over z, y, x), tp: 2 (over core).
Axes of the slice: x: 2, y: 2, z: 4, core: 2. Of those that a mesh axis runs over, the one named last changes fastest.
Arguments:
- tokens: bfloat16 [4096, 2048], P(('sp', 'tp')), may hold values from -6 to 6
- norm_gain: float32 [2048], replicated, may hold values from 0.1 to 1.9
- w_query: bfloat16 [2048, 1024], P('sp', 'tp'), may hold values from -0.125 to 0.125
- w_forget: bfloat16 [2048, 1024], P('sp', 'tp'), may hold values from -0.125 to 0.125
- w_value: bfloat16 [2048, 1024], P('sp', 'tp'), may hold values from -0.125 to 0.125
- w_outgate: bfloat16 [2048, 1024], P('sp', 'tp'), may hold values from -0.125 to 0.125
- leak: float32 [1024], P('tp'), may hold values from 4.8828126e-05 to 0.00024414062
- decay_shift: float32 [4096, 1024], P('sp', 'tp'), may hold values from -1 to 0
- head_gain: float32 [128], replicated, may hold values from 0.1 to 1.9
- w_glu_value: bfloat16 [2048, 2048], P('sp', 'tp'), may hold values from -0.125 to 0.125
- w_glu_gate: bfloat16 [2048, 2048], P('sp', 'tp'), may hold values from -0.125 to 0.125
- conv_kernel: float32 [31, 2048], P(None, 'tp'), may hold values from -20 to 20
- ln_gain: float32 [2048], P('tp'), may hold values from 0.1 to 1.9
- ln_bias: float32 [2048], P('tp'), may hold values from -3 to 3
- w_out_rec: bfloat16 [1024, 2048], P('tp', 'sp'), may hold values from -0.125 to 0.125
- w_out_conv: bfloat16 [2048, 2048], P('tp', 'sp'), may hold values from -0.09375 to 0.09375
Outputs:
- mixed: bfloat16 [4096, 2048], P(('sp', 'tp'))
All inputs are finite; a program needn't handle non-finite values.
Results may differ from a plain program's by a relative error of at most 0.019.
Values may be sent and summed in bfloat16 or wider, within the bound.
A program may use at most 64 MiB of HBM per device.

v0:
```python
import jax
import jax.numpy as jnp
from jax import lax
from jax.sharding import PartitionSpec as P

HEAD_K = 128
HEAD_V = 128
KERNEL = 31
BLOCK = 64
exact_precision = lax.Precision.HIGHEST


def prefix(value, axis, combine, identity):
    peers, position = (lax.axis_size(axis), lax.axis_index(axis))
    everything = jax.tree.map(
        lambda part, kind: lax.all_gather(part.astype(kind), axis),
        value,
        (jnp.bfloat16, jnp.bfloat16),
    )
    start = jax.tree.map(
        lambda part, zero: jnp.broadcast_to(jnp.asarray(zero, part.dtype), part.shape),
        value,
        identity,
    )

    def turn(k, before):
        reached = k < position
        new = combine(
            before, jax.tree.map(lambda part, own: part[k].astype(own.dtype), everything, value)
        )
        return jax.tree.map(lambda a, b: jnp.where(reached, a, b), new, before)

    return lax.fori_loop(0, peers, turn, start)


def from_behind(value, axis, steps):
    count = lax.axis_size(axis)
    initial, last = (max(0, -steps), min(count, count - steps))
    return lax.ppermute(value, axis, [(source, source + steps) for source in range(initial, last)])


def normalize(row_block, norm_gain):
    values_in = row_block.astype(jnp.float32)
    row_scale = lax.rsqrt(jnp.mean(values_in * values_in, axis=1, keepdims=True) + 1e-06)
    return (values_in * row_scale * norm_gain).astype(jnp.bfloat16)


def combine_states(earlier, later):
    return (earlier[0] + later[0], jnp.exp(later[0])[..., None] * earlier[1] + later[1])


def local_recurrence(queries, in_gate, payload_matrix_lines, log_decay):
    row_count, head_count, key_width = queries.shape
    value_width = payload_matrix_lines.shape[2]
    block_count = row_count // BLOCK

    def split_blocks(tensor):
        return tensor.reshape(block_count, BLOCK, head_count, tensor.shape[-1])

    q_blocks = split_blocks(queries)
    k_blocks = split_blocks(in_gate)
    v_blocks = split_blocks(payload_matrix_lines)
    cumulative_sum = jnp.cumsum(split_blocks(log_decay), axis=1)
    causal = jnp.tril(jnp.ones((BLOCK, BLOCK), jnp.float32))
    scores = jnp.einsum(
        "nthk,nshk->nhts",
        q_blocks * jnp.exp(cumulative_sum),
        k_blocks * jnp.exp(-cumulative_sum),
        precision=exact_precision,
    )
    within = jnp.einsum("nhts,nshv->nthv", scores * causal, v_blocks, precision=exact_precision)
    block_finish = cumulative_sum[:, -1]
    contrib = jnp.einsum(
        "nshk,nshv->nhkv",
        k_blocks * jnp.exp(block_finish[:, None] - cumulative_sum),
        v_blocks,
        precision=exact_precision,
    )

    def advance(carried_in, inputs):
        state_list, before = carried_in
        query_block, column_block, e_block, added_terms = inputs
        carried_state = jnp.einsum(
            "aub,ubd->aud",
            query_block * jnp.exp(column_block),
            state_list,
            precision=exact_precision,
        )
        device_query = query_block * jnp.exp(column_block + before[None])
        state_list = jnp.exp(e_block)[..., None] * state_list + added_terms
        return ((state_list, before + e_block), (carried_state, device_query))

    initial = (
        jnp.zeros((head_count, key_width, value_width), jnp.float32),
        jnp.zeros((head_count, key_width), jnp.float32),
    )
    (state_list, totals), (carried_state, device_query) = lax.scan(
        advance, initial, (q_blocks, cumulative_sum, block_finish, contrib)
    )
    recurrence_step = (within + carried_state).reshape(row_count, head_count, value_width)
    return (
        recurrence_step,
        device_query.reshape(row_count, head_count, key_width),
        state_list,
        totals,
    )


def on_device(
    tokens,
    norm_gain,
    w_query,
    w_forget,
    w_value,
    w_outgate,
    leak,
    decay_shift,
    head_gain,
    w_glu_value,
    w_glu_gate,
    conv_kernel,
    ln_gain,
    ln_bias,
    w_out_rec,
    w_out_conv,
):
    widths = [
        w_query.shape[1],
        w_forget.shape[1],
        w_value.shape[1],
        w_outgate.shape[1],
        w_glu_value.shape[1],
        w_glu_gate.shape[1],
    ]
    gathered = (
        lax.all_gather(w_query, "sp", axis=0, tiled=True),
        lax.all_gather(w_forget, "sp", axis=0, tiled=True),
        lax.all_gather(w_value, "sp", axis=0, tiled=True),
        lax.all_gather(w_outgate, "sp", axis=0, tiled=True),
        lax.all_gather(w_glu_value, "sp", axis=0, tiled=True),
        lax.all_gather(w_glu_gate, "sp", axis=0, tiled=True),
        lax.all_gather(w_out_rec, "sp", axis=1, tiled=True),
        lax.all_gather(w_out_conv, "sp", axis=1, tiled=True),
    )
    full_in = gathered[:6]
    out_rec = gathered[6]
    out_conv = gathered[7]
    normed = normalize(lax.all_gather(tokens, "tp", axis=0, tiled=True), norm_gain)
    joined = jnp.concatenate(
        [
            jnp.dot(normed, weight, preferred_element_type=jnp.float32).astype(jnp.bfloat16)
            for weight in full_in
        ],
        axis=1,
    )
    projections = []
    column = 0
    for width_now in widths:
        projections.append(joined[:, column : column + width_now])
        column = column + width_now
    query_pre, forget_pre, value_pre, gate_pre, glu_value_pre, glu_gate_pre = projections
    row_count = query_pre.shape[0]
    head_count = query_pre.shape[1] // HEAD_K
    queries = jax.nn.silu(query_pre.astype(jnp.float32))
    in_gate = leak * jax.nn.sigmoid(-forget_pre.astype(jnp.float32))
    log_decay = jnp.log1p(-in_gate) + decay_shift
    recurrence_step, device_query, state_list, totals = local_recurrence(
        queries.reshape(row_count, head_count, HEAD_K),
        in_gate.reshape(row_count, head_count, HEAD_K),
        value_pre.astype(jnp.float32).reshape(row_count, head_count, HEAD_V),
        log_decay.reshape(row_count, head_count, HEAD_K),
    )
    _, incoming_state = prefix(
        (totals, state_list),
        "sp",
        combine_states,
        (jnp.zeros_like(totals), jnp.zeros_like(state_list)),
    )
    recurrence_step = recurrence_step + jnp.einsum(
        "aub,ubd->aud", device_query, incoming_state, precision=exact_precision
    )
    scaling = lax.rsqrt(jnp.mean(recurrence_step * recurrence_step, axis=2, keepdims=True) + 1e-06)
    gate_act = jax.nn.silu(gate_pre.astype(jnp.float32)).reshape(row_count, head_count, HEAD_V)
    head_out = (
        (recurrence_step * scaling * head_gain * gate_act)
        .reshape(row_count, head_count * HEAD_V)
        .astype(jnp.bfloat16)
    )
    glu = (
        glu_value_pre.astype(jnp.float32) * jax.nn.sigmoid(glu_gate_pre.astype(jnp.float32))
    ).astype(jnp.bfloat16)
    left_rim = from_behind(glu[row_count - (KERNEL - 1) :], "sp", 1)
    extended = jnp.concatenate([left_rim, glu], axis=0).astype(jnp.float32)

    def add_tap(tap_index, accum):
        taps = lax.dynamic_slice_in_dim(conv_kernel, tap_index, 1, 0)
        return accum + taps * lax.dynamic_slice_in_dim(extended, tap_index, row_count, 0)

    conv_sum = lax.fori_loop(0, KERNEL, add_tap, jnp.zeros((row_count, glu.shape[1]), jnp.float32))
    channel_count = conv_sum.shape[1] * lax.axis_size("tp")
    sum_rows, square_rows = lax.psum(
        (
            jnp.sum(conv_sum, axis=1, keepdims=True),
            jnp.sum(conv_sum * conv_sum, axis=1, keepdims=True),
        ),
        "tp",
    )
    row_mean = sum_rows / channel_count
    centered = conv_sum - row_mean
    row_var = square_rows / channel_count - row_mean * row_mean
    conv_out = jax.nn.silu(centered * lax.rsqrt(row_var + 1e-05) * ln_gain + ln_bias).astype(
        jnp.bfloat16
    )
    return lax.psum_scatter(
        (
            jnp.dot(head_out, out_rec, preferred_element_type=jnp.float32)
            + jnp.dot(conv_out, out_conv, preferred_element_type=jnp.float32)
        ).astype(jnp.bfloat16),
        "tp",
        scatter_dimension=0,
        tiled=True,
    )


def solution(mesh):
    placed = (
        P(("sp", "tp"), None),
        P(),
        P("sp", "tp"),
        P("sp", "tp"),
        P("sp", "tp"),
        P("sp", "tp"),
        P("tp"),
        P("sp", "tp"),
        P(),
        P("sp", "tp"),
        P("sp", "tp"),
        P(None, "tp"),
        P("tp"),
        P("tp"),
        P("tp", "sp"),
        P("tp", "sp"),
    )
    return jax.shard_map(
        on_device, mesh=mesh, in_specs=placed, out_specs=P(("sp", "tp"), None), check_vma=False
    )
```

profile of v0, /device:TPU:0, one launch (start us, length us, event | category | flops | bytes accessed | tf_op | source)
XLA Modules:
  0.0 657.1 jit_solution(7365507671859252702)
XLA Ops:
  10.0 10.7 %all-gather.14.cloned.1.call-done = bf16[256,2048]{1,0:T(8,128)(2,1)} async-done(((bf16[128,2048]{1,0:T(8,128)(2,1)}), bf16[256,2048]{1,0:T(8,128)(2,1)}) %all-gather.14.cloned.1.call-update) | async-done | bytes 1048592 | tf_op jit(solution)/shard_map/all_gather | solution.py:148
  22.2 62.8 %all-gather.20.cloned.1.call-done = bf16[2048,512]{1,0:T(8,128)(2,1)} async-done(((bf16[128,512]{1,0:T(8,128)(2,1)}), bf16[2048,512]{1,0:T(8,128)(2,1)}) %all-gather.20.cloned.1.call-update) | async-done | bytes 2097168 | tf_op jit(solution)/shard_map/all_gather | solution.py:137
  85.0 2.9 log-plus-one_add_fusion
  88.5 58.5 %all-gather.18.cloned.1.call-done = bf16[2048,512]{1,0:T(8,128)(2,1)} async-done(((bf16[128,512]{1,0:T(8,128)(2,1)}), bf16[2048,512]{1,0:T(8,128)(2,1)}) %all-gather.18.cloned.1.call-update) | async-done | bytes 2097168 | tf_op jit(solution)/shard_map/all_gather | solution.py:136
  147.0 2.8 divide_multiply_fusion.1
  150.0 58.9 %all-gather.16.cloned.1.call-done = bf16[2048,512]{1,0:T(8,128)(2,1)} async-done(((bf16[128,512]{1,0:T(8,128)(2,1)}), bf16[2048,512]{1,0:T(8,128)(2,1)}) %all-gather.16.cloned.1.call-update) | async-done | bytes 2097168 | tf_op jit(solution)/shard_map/all_gather | solution.py:138
  208.8 2.7 convolution_convert_fusion.5
  213.8 7.8 %while.45 = (s32[]{:T(128)}, f32[4,128,128]{2,1,0:T(8,128)S(1)}, f32[4,128]{1,0:T(4,128)S(1)}, f32[4,64,4,128]{3,1,2,0:T(8,128)}, f32[4,64,4,128]{3,1,0,2:T(8,12...) while((s32[]{:T(128)}, f32[4,128,128]{2,1,0:T(8,128)S(1)}, ...), condition=%wide.region_3.4_spmd.clone, body=%wide.region_2.3_spmd.clone.sunk | while | flops 50693120 | bytes 2374789 | solution.py:97
  225.3 38.8 %all-gather.2 = bf16[16,4,128]{2,1,0:T(4,128)(2,1)S(1)} all-gather(bf16[1,4,128]{2,1,0:T(4,128)(2,1)S(1)} %convert_bitcast_fusion), channel_id=2, replica_groups=mesh['sp'=16,'tp'=2] {'sp'}, dimensions={0}, use_global_device_ids=true | all-gather | bytes 17408 | tf_op jit(solution)/shard_map/all_gather | solution.py:16
  266.8 3.9 all-gather.22.cloned.1.call-done
  270.7 2.8 divide_multiply_fusion
  273.7 58.9 %all-gather.32.cloned.1.call-done = bf16[64,128,128]{2,1,0:T(8,128)(2,1)} async-done(((bf16[4,128,128]{2,1,0:T(8,128)(2,1)}), bf16[64,128,128]{2,1,0:T(8,128)(2,1)}) %all-gather.32.cloned.1.call-update) | async-done | bytes 2097168 | tf_op jit(solution)/shard_map/all_gather | solution.py:16
  332.6 18.4 %while.46 = (s32[]{:T(128)}, f32[4,128,128]{2,1,0:T(8,128)S(1)}, s32[]{:T(128)}, bf16[16,4,128]{2,1,0:T(4,128)(2,1)S(1)}, bf16[16,4,128,128]{3,2,1,0:T(8,128)(2,1)}, /*index=5*/s32[]{:T(128)}, s32[]{:T(128)}) while((s32[]{:T(128)}, f32[4,128,128]{2,1,0:T(8,128)S(1)}, s32[]{:T(128)}, bf16[16,4,128]{2,1,0:T(4,128)(2,1)S(1)}, ...), condition=%wide.region_5.6_spmd.clone, body=%wide.region_4.5_spmd.clone.sunk | while | flops 328196 | bytes 660585 | solution.py:33
  352.7 57.1 %all-gather.26.cloned.1.call-done = bf16[2048,1024]{1,0:T(8,128)(2,1)} async-done(((bf16[128,1024]{1,0:T(8,128)(2,1)}), bf16[2048,1024]{1,0:T(8,128)(2,1)}) %all-gather.26.cloned.1.call-update) | async-done | bytes 4194320 | tf_op jit(solution)/shard_map/all_gather | solution.py:140
  409.8 4.8 fusion.22
  414.6 72.2 %all-gather.28.cloned.1.call-done = bf16[2048,1024]{1,0:T(8,128)(2,1)} async-done(((bf16[128,1024]{1,0:T(8,128)(2,1)}), bf16[2048,1024]{1,0:T(8,128)(2,1)}) %all-gather.28.cloned.1.call-update) | async-done | bytes 4194320 | tf_op jit(solution)/shard_map/all_gather | solution.py:141
  486.8 4.2 fusion.21
  491.0 3.5 collective-permute-start
  496.4 40.1 %while.47 = (s32[]{:T(128)}, f32[256,1024]{1,0:T(8,128)S(1)}, f32[31,1024]{1,0:T(8,128)}, f32[286,1024]{1,0:T(8,128)S(1)}, s32[]{:T(128)}, /*index=5*/s32[]{:T(128)}) while((s32[]{:T(128)}, f32[256,1024]{1,0:T(8,128)S(1)}, f32[31,1024]{1,0:T(8,128)}, f32[286,1024]{1,0:T(8,128)S(1)}, s32[]{:T(128)}, /*index=5*/s32[]{:T(128)}) %tuple.92), condition=%wide.region_8.9_spmd.clone, body=%wide.region_7.8_spmd.clone.sunk | while | flops 786435 | bytes 3158103 | solution.py:199
  539.2 37.6 %all-gather.30.cloned.1.call-done = bf16[1024,2048]{1,0:T(8,128)(2,1)} async-done(((bf16[1024,128]{1,0:T(8,128)(2,1)}), bf16[1024,2048]{1,0:T(8,128)(2,1)}) %all-gather.30.cloned.1.call-update) | async-done | bytes 4194320 | tf_op jit(solution)/shard_map/all_gather | solution.py:143
  576.8 3.7 fusion.32
  580.5 60.0 %all-gather.24.cloned.1.call-done = bf16[512,2048]{1,0:T(8,128)(2,1)} async-done(((bf16[512,128]{1,0:T(8,128)(2,1)}), bf16[512,2048]{1,0:T(8,128)(2,1)}) %all-gather.24.cloned.1.call-update) | async-done | bytes 2097168 | tf_op jit(solution)/shard_map/all_gather | solution.py:142
  640.5 3.3 fusion.11
  643.9 6.7 %reduce-scatter.2.cloned.1.call-done = bf16[128,2048]{1,0:T(8,128)(2,1)} async-done(((bf16[256,2048]{1,0:T(8,128)(2,1)}), bf16[128,2048]{1,0:T(8,128)(2,1)}) %reduce-scatter.2.cloned.1.call-update) | async-done | bytes 524304 | tf_op jit(solution)/shard_map/reduce_scatter | solution.py:214
  (183 shorter events, 85.5 us)
Async XLA Ops:
  6.5 78.5 %copy-start.3 = (f32[2048]{0:T(1024)S(1)}, f32[2048]{0:T(1024)}, u32[]{:S(2)}) copy-start(f32[2048]{0:T(1024)} %param.23) | copy-start | bytes 24580
  6.5 78.5 %copy-start.6 = (f32[512]{0:T(512)S(1)}, f32[512]{0:T(512)}, u32[]{:S(2)}) copy-start(f32[512]{0:T(512)} %param.28) | copy-start | bytes 6148
  6.5 78.5 %copy-start.2 = (f32[256,512]{1,0:T(8,128)S(1)}, f32[256,512]{1,0:T(8,128)}, u32[]{:S(2)}) copy-start(f32[256,512]{1,0:T(8,128)} %param.29) | copy-start | bytes 1572868
  6.5 14.1 %all-gather.14.cloned.1.call-start = ((), (), s32[]{:S(2)}) async-start(), calls=%async_computation.1 | async-start | bytes 1572864 | tf_op jit(solution)/shard_map/all_gather | solution.py:148
  7.3 77.8 %all-gather.20.cloned.1.call-start = ((), (), s32[]{:S(2)}) async-start(), calls=%async_computation.4 | async-start | bytes 2228224 | tf_op jit(solution)/shard_map/all_gather | solution.py:137
  8.0 139.0 %all-gather.18.cloned.1.call-start = ((), (), s32[]{:S(2)}) async-start(), calls=%async_computation.3 | async-start | bytes 2228224 | tf_op jit(solution)/shard_map/all_gather | solution.py:136
  8.7 200.1 %all-gather.16.cloned.1.call-start = ((), (), s32[]{:S(2)}) async-start(), calls=%async_computation.2 | async-start | bytes 2228224 | tf_op jit(solution)/shard_map/all_gather | solution.py:138
  9.3 261.4 %all-gather.22.cloned.1.call-start = ((), (), s32[]{:S(2)}) async-start(), calls=%async_computation.5 | async-start | bytes 2228224 | tf_op jit(solution)/shard_map/all_gather | solution.py:139
  9.9 322.7 %all-gather.32.cloned.1.call-start = ((), (), s32[]{:S(2)}) async-start(), calls=%async_computation.11 | async-start | bytes 2228224 | tf_op jit(solution)/shard_map/all_gather | solution.py:16
  221.7 44.5 %copy-start = (f32[4,64,4,128]{3,1,2,0:T(8,128)S(1)}, f32[4,64,4,128]{3,1,2,0:T(8,128)}, u32[]{:S(2)}) copy-start(f32[4,64,4,128]{3,1,2,0:T(8,128)} %get-tuple-element.228) | copy-start | bytes 1572868
  222.4 187.4 %all-gather.26.cloned.1.call-start = ((), (), s32[]{:S(2)}) async-start(), calls=%async_computation.7 | async-start | bytes 4456448 | tf_op jit(solution)/shard_map/all_gather | solution.py:140
  223.1 263.6 %all-gather.28.cloned.1.call-start = ((), (), s32[]{:S(2)}) async-start(), calls=%async_computation.8 | async-start | bytes 4456448 | tf_op jit(solution)/shard_map/all_gather | solution.py:141
  223.9 352.9 %all-gather.30.cloned.1.call-start = ((), (), s32[]{:S(2)}) async-start(), calls=%async_computation.9 | async-start | bytes 4456448 | tf_op jit(solution)/shard_map/all_gather | solution.py:143
  224.6 415.9 %all-gather.24.cloned.1.call-start = ((), (), s32[]{:S(2)}) async-start(), calls=%async_computation.6 | async-start | bytes 2228224 | tf_op jit(solution)/shard_map/all_gather | solution.py:142
  225.2 425.4 %reduce-scatter.2.cloned.1.call-start = ((), (), s32[]{:S(2)}) async-start(), calls=%async_computation.10 | async-start | bytes 1572864 | tf_op jit(solution)/shard_map/reduce_scatter | solution.py:214
  414.6 79.9 %copy-start.1 = (f32[128]{0:T(128)S(1)}, f32[128]{0:T(128)}, u32[]{:S(2)}) copy-start(f32[128]{0:T(128)} %param.30) | copy-start | bytes 1540
  491.0 5.2 collective-permute-start
  496.4 80.4 %copy-start.4 = (f32[1024]{0:T(1024)S(1)}, f32[1024]{0:T(1024)}, u32[]{:S(2)}) copy-start(f32[1024]{0:T(1024)} %param.35) | copy-start | bytes 12292
  496.4 80.4 %copy-start.5 = (f32[1024]{0:T(1024)S(1)}, f32[1024]{0:T(1024)}, u32[]{:S(2)}) copy-start(f32[1024]{0:T(1024)} %param.34) | copy-start | bytes 12292
Sparse Core Ops, SparseCore 0:
  8.9 11.7 all-gather.13
  23.4 61.5 all-gather.19
  87.8 59.1 all-gather.17
  149.6 59.1 all-gather.15
  211.5 59.2 all-gather.21
  273.4 59.1 all-gather.31
  335.3 74.3 all-gather.25
  412.5 74.1 all-gather.27
  489.5 87.3 all-gather.29
  579.4 61.1 all-gather.23
  644.0 6.5 reduce-scatter.1
where the time goes:
time: 660 us; the launch traced here: 657 us
  waiting for transfers between devices  495 us (75%)
  blocking collectives  41.3 us (6%)
  other arithmetic  41 us (6%)
  matrix products  36.4 us (6%)
  local copies, waits for them, and re-layouts  25 us (4%)
  between operations  13.6 us (2%)
    all_gather x1, waiting for transfers between devices, on_device(): lax.all_gather(w_glu_gate, 'sp', axis=0, tiled=True)  72.2 us
    all_gather x1, waiting for transfers between devices, on_device(): lax.all_gather(w_forget, 'sp', axis=0, tiled=True)  62.8 us
    all_gather x1, waiting for transfers between devices, on_device(): lax.all_gather(w_out_rec, 'sp', axis=1, tiled=True)  60 us
    all_gather x1, waiting for transfers between devices, on_device(): lax.all_gather(w_value, 'sp', axis=0, tiled=True)  58.9 us
    all_gather x1, waiting for transfers between devices, prefix(): lax.all_gather(part.astype(kind), axis)  58.9 us
    all_gather x1, waiting for transfers between devices, on_device(): lax.all_gather(w_query, 'sp', axis=0, tiled=True)  58.5 us
    all_gather x1, waiting for transfers between devices, on_device(): lax.all_gather(w_glu_value, 'sp', axis=0, tiled=True)  57.1 us
    all_gather x1, blocking collectives, prefix(): lax.all_gather(part.astype(kind), axis)  38.8 us
  transfers between devices with their start and end apart: 12, of which 12 were waited for; matrix products, arithmetic and copies ran while one was open for 15% of the time, Pallas kernels for 0%

commit v1 on v0

--- a/solution.py
+++ b/solution.py
@@ -139,7 +139,9 @@
         lax.all_gather(w_outgate, "sp", axis=0, tiled=True),
         lax.all_gather(w_glu_value, "sp", axis=0, tiled=True),
         lax.all_gather(w_glu_gate, "sp", axis=0, tiled=True),
-        lax.all_gather(w_out_rec, "sp", axis=1, tiled=True),
+        jnp.concatenate(
+            lax.all_to_all(jnp.stack([w_out_rec] * lax.axis_size("sp")), "sp", 0, 0), axis=1
+        ),
         lax.all_gather(w_out_conv, "sp", axis=1, tiled=True),
     )
     full_in = gathered[:6]

time: 660 us -> 621 us (0.941)
  waiting for transfers between devices: 495 us -> 408 us
  blocking collectives: 41.3 us -> 83.9 us
    all_gather x1 -> x0, waiting for transfers between devices: 60 us -> none  [on_device(): lax.all_gather(w_out_rec, 'sp', axis=1, tiled=True)]
    all_gather x1, blocking collectives: 38.8 us -> 81.5 us  [prefix(): lax.all_gather(part.astype(kind), axis)]
    all_gather x1, waiting for transfers between devices: 58.9 us -> 36.4 us  [prefix(): lax.all_gather(part.astype(kind), axis)]
  transfers between devices with their start and end apart: 12 -> 12, of which waited for: 12 -> 10; matrix products, arithmetic and copies ran while one was open for 15% -> 16% of each run, Pallas kernels for 0% -> 0%
where the time goes in v1:
time: 621 us; the launch traced here: 618 us
  waiting for transfers between devices  408 us (66%)
  blocking collectives  83.9 us (14%)
  other arithmetic  41 us (7%)
  matrix products  34.7 us (6%)
  local copies, waits for them, and re-layouts  26.7 us (4%)
  between operations  13.9 us (2%)
  starting transfers between devices  8.48 us (1%)
    all_gather x1, blocking collectives, prefix(): lax.all_gather(part.astype(kind), axis)  81.5 us
    all_gather x1, waiting for transfers between devices, on_device(): lax.all_gather(w_glu_gate, 'sp', axis=0, tiled=True)  72.2 us
    all_gather x1, waiting for transfers between devices, on_device(): lax.all_gather(w_forget, 'sp', axis=0, tiled=True)  62.8 us
    all_gather x1, waiting for transfers between devices, on_device(): lax.all_gather(w_value, 'sp', axis=0, tiled=True)  59.2 us
    all_gather x1, waiting for transfers between devices, on_device(): lax.all_gather(w_query, 'sp', axis=0, tiled=True)  58.5 us
    all_gather x1, waiting for transfers between devices, on_device(): lax.all_gather(w_glu_value, 'sp', axis=0, tiled=True)  57.1 us
    all_gather x1, waiting for transfers between devices, on_device(): lax.all_gather(w_out_conv, 'sp', axis=1, tiled=True)  37.9 us
    all_gather x1, waiting for transfers between devices, prefix(): lax.all_gather(part.astype(kind), axis)  36.4 us
  transfers between devices with their start and end apart: 12, of which 10 were waited for; matrix products, arithmetic and copies ran while one was open for 16% of the time, Pallas kernels for 0%

profile of v1, /device:TPU:0, one launch (start us, length us, event | category | flops | bytes accessed | tf_op | source)
XLA Modules:
  0.0 618.5 jit_solution(4115681683504254443)
XLA Ops:
  10.0 10.7 %all-gather.13.cloned.1.call-done = bf16[256,2048]{1,0:T(8,128)(2,1)} async-done(((bf16[128,2048]{1,0:T(8,128)(2,1)}), bf16[256,2048]{1,0:T(8,128)(2,1)}) %all-gather.13.cloned.1.call-update) | async-done | bytes 1048592 | tf_op jit(solution)/shard_map/all_gather | solution.py:150
  22.2 62.8 %all-gather.19.cloned.1.call-done = bf16[2048,512]{1,0:T(8,128)(2,1)} async-done(((bf16[128,512]{1,0:T(8,128)(2,1)}), bf16[2048,512]{1,0:T(8,128)(2,1)}) %all-gather.19.cloned.1.call-update) | async-done | bytes 2097168 | tf_op jit(solution)/shard_map/all_gather | solution.py:137
  85.0 2.9 log-plus-one_add_fusion
  88.5 58.5 %all-gather.17.cloned.1.call-done = bf16[2048,512]{1,0:T(8,128)(2,1)} async-done(((bf16[128,512]{1,0:T(8,128)(2,1)}), bf16[2048,512]{1,0:T(8,128)(2,1)}) %all-gather.17.cloned.1.call-update) | async-done | bytes 2097168 | tf_op jit(solution)/shard_map/all_gather | solution.py:136
  147.0 2.4 divide_multiply_fusion.1
  149.6 59.2 %all-gather.15.cloned.1.call-done = bf16[2048,512]{1,0:T(8,128)(2,1)} async-done(((bf16[128,512]{1,0:T(8,128)(2,1)}), bf16[2048,512]{1,0:T(8,128)(2,1)}) %all-gather.15.cloned.1.call-update) | async-done | bytes 2097168 | tf_op jit(solution)/shard_map/all_gather | solution.py:138
  208.8 2.7 convolution_convert_fusion.5
  213.8 7.8 %while.45 = (s32[]{:T(128)}, f32[4,128,128]{2,1,0:T(8,128)S(1)}, f32[4,128]{1,0:T(4,128)S(1)}, f32[4,64,4,128]{3,1,2,0:T(8,128)}, f32[4,64,4,128]{3,1,0,2:T(8,12...) while((s32[]{:T(128)}, f32[4,128,128]{2,1,0:T(8,128)S(1)}, ...), condition=%wide.region_3.4_spmd.clone, body=%wide.region_2.3_spmd.clone.sunk | while | flops 50693120 | bytes 2374789 | solution.py:97
  225.5 4.6 all-to-all-start
  231.0 81.5 %all-gather.2 = bf16[16,4,128]{2,1,0:T(4,128)(2,1)S(1)} all-gather(bf16[1,4,128]{2,1,0:T(4,128)(2,1)S(1)} %convert_bitcast_fusion), channel_id=2, replica_groups=mesh['sp'=16,'tp'=2] {'sp'}, dimensions={0}, use_global_device_ids=true | all-gather | bytes 17408 | tf_op jit(solution)/shard_map/all_gather | solution.py:16
  314.1 2.8 divide_multiply_fusion
  317.1 36.4 %all-gather.29.cloned.1.call-done = bf16[64,128,128]{2,1,0:T(8,128)(2,1)} async-done(((bf16[4,128,128]{2,1,0:T(8,128)(2,1)}), bf16[64,128,128]{2,1,0:T(8,128)(2,1)}) %all-gather.29.cloned.1.call-update) | async-done | bytes 2097168 | tf_op jit(solution)/shard_map/all_gather | solution.py:16
  353.5 18.4 %while.46 = (s32[]{:T(128)}, f32[4,128,128]{2,1,0:T(8,128)S(1)}, s32[]{:T(128)}, bf16[16,4,128]{2,1,0:T(4,128)(2,1)S(1)}, bf16[16,4,128,128]{3,2,1,0:T(8,128)(2,1)}, /*index=5*/s32[]{:T(128)}, s32[]{:T(128)}) while((s32[]{:T(128)}, f32[4,128,128]{2,1,0:T(8,128)S(1)}, s32[]{:T(128)}, bf16[16,4,128]{2,1,0:T(4,128)(2,1)S(1)}, ...), condition=%wide.region_5.6_spmd.clone, body=%wide.region_4.5_spmd.clone.sunk | while | flops 328196 | bytes 660585 | solution.py:33
  373.6 57.1 %all-gather.23.cloned.1.call-done = bf16[2048,1024]{1,0:T(8,128)(2,1)} async-done(((bf16[128,1024]{1,0:T(8,128)(2,1)}), bf16[2048,1024]{1,0:T(8,128)(2,1)}) %all-gather.23.cloned.1.call-update) | async-done | bytes 4194320 | tf_op jit(solution)/shard_map/all_gather | solution.py:140
  430.7 4.8 fusion.22
  435.5 72.2 %all-gather.25.cloned.1.call-done = bf16[2048,1024]{1,0:T(8,128)(2,1)} async-done(((bf16[128,1024]{1,0:T(8,128)(2,1)}), bf16[2048,1024]{1,0:T(8,128)(2,1)}) %all-gather.25.cloned.1.call-update) | async-done | bytes 4194320 | tf_op jit(solution)/shard_map/all_gather | solution.py:141
  507.7 3.9 fusion.21
  511.6 3.5 collective-permute-start
  517.0 40.1 %while.47 = (s32[]{:T(128)}, f32[256,1024]{1,0:T(8,128)S(1)}, f32[31,1024]{1,0:T(8,128)}, f32[286,1024]{1,0:T(8,128)S(1)}, s32[]{:T(128)}, /*index=5*/s32[]{:T(128)}) while((s32[]{:T(128)}, f32[256,1024]{1,0:T(8,128)S(1)}, f32[31,1024]{1,0:T(8,128)}, f32[286,1024]{1,0:T(8,128)S(1)}, s32[]{:T(128)}, /*index=5*/s32[]{:T(128)}) %tuple.92), condition=%wide.region_8.9_spmd.clone, body=%wide.region_7.8_spmd.clone.sunk | while | flops 786435 | bytes 3158103 | solution.py:201
  557.4 2.5 all-reduce
  559.8 37.9 %all-gather.27.cloned.1.call-done = bf16[1024,2048]{1,0:T(8,128)(2,1)} async-done(((bf16[1024,128]{1,0:T(8,128)(2,1)}), bf16[1024,2048]{1,0:T(8,128)(2,1)}) %all-gather.27.cloned.1.call-update) | async-done | bytes 4194320 | tf_op jit(solution)/shard_map/all_gather | solution.py:145
  597.8 3.7 fusion.32
  601.5 3.3 fusion.11
  604.9 6.7 %reduce-scatter.2.cloned.1.call-done = bf16[128,2048]{1,0:T(8,128)(2,1)} async-done(((bf16[256,2048]{1,0:T(8,128)(2,1)}), bf16[128,2048]{1,0:T(8,128)(2,1)}) %reduce-scatter.2.cloned.1.call-update) | async-done | bytes 524304 | tf_op jit(solution)/shard_map/reduce_scatter | solution.py:216
  (194 shorter events, 83.1 us)
Async XLA Ops:
  6.5 78.5 %copy-start.7 = (f32[2048]{0:T(1024)S(1)}, f32[2048]{0:T(1024)}, u32[]{:S(2)}) copy-start(f32[2048]{0:T(1024)} %param.23) | copy-start | bytes 24580
  6.5 78.5 %copy-start.11 = (f32[512]{0:T(512)S(1)}, f32[512]{0:T(512)}, u32[]{:S(2)}) copy-start(f32[512]{0:T(512)} %param.28) | copy-start | bytes 6148
  6.5 78.5 %copy-start.6 = (f32[256,512]{1,0:T(8,128)S(1)}, f32[256,512]{1,0:T(8,128)}, u32[]{:S(2)}) copy-start(f32[256,512]{1,0:T(8,128)} %param.29) | copy-start | bytes 1572868
  6.5 14.1 %all-gather.13.cloned.1.call-start = ((), (), s32[]{:S(2)}) async-start(), calls=%async_computation.2 | async-start | bytes 1572864 | tf_op jit(solution)/shard_map/all_gather | solution.py:150
  7.3 77.8 %all-gather.19.cloned.1.call-start = ((), (), s32[]{:S(2)}) async-start(), calls=%async_computation.5 | async-start | bytes 2228224 | tf_op jit(solution)/shard_map/all_gather | solution.py:137
  8.0 139.0 %all-gather.17.cloned.1.call-start = ((), (), s32[]{:S(2)}) async-start(), calls=%async_computation.4 | async-start | bytes 2228224 | tf_op jit(solution)/shard_map/all_gather | solution.py:136
  8.7 200.1 %all-gather.15.cloned.1.call-start = ((), (), s32[]{:S(2)}) async-start(), calls=%async_computation.3 | async-start | bytes 2228224 | tf_op jit(solution)/shard_map/all_gather | solution.py:138
  9.3 304.8 %all-gather.21.cloned.1.call-start = ((), (), s32[]{:S(2)}) async-start(), calls=%async_computation.6 | async-start | bytes 2228224 | tf_op jit(solution)/shard_map/all_gather | solution.py:139
  9.9 343.6 %all-gather.29.cloned.1.call-start = ((), (), s32[]{:S(2)}) async-start(), calls=%async_computation.11 | async-start | bytes 2228224 | tf_op jit(solution)/shard_map/all_gather | solution.py:16
  88.0 59.0 %copy-start.1 = (bf16[256,2048]{1,0:T(8,128)(2,1)S(1)}, bf16[256,2048]{1,0:T(8,128)(2,1)}, u32[]{:S(2)}) copy-start(bf16[256,2048]{1,0:T(8,128)(2,1)} %all-gather.13.cloned.1.call-done) | copy-start | bytes 3145732
  213.8 10.0 %copy-start.4 = (bf16[512,128]{1,0:T(8,128)(2,1)S(1)}, bf16[512,128]{1,0:T(8,128)(2,1)}, u32[]{:S(2)}) copy-start(bf16[512,128]{1,0:T(8,128)(2,1)} %param.36) | copy-start | bytes 393220
  222.3 208.4 %all-gather.23.cloned.1.call-start = ((), (), s32[]{:S(2)}) async-start(), calls=%async_computation.7 | async-start | bytes 4456448 | tf_op jit(solution)/shard_map/all_gather | solution.py:140
  223.1 284.6 %all-gather.25.cloned.1.call-start = ((), (), s32[]{:S(2)}) async-start(), calls=%async_computation.8 | async-start | bytes 4456448 | tf_op jit(solution)/shard_map/all_gather | solution.py:141
  225.5 86.9 %copy-start = (f32[4,64,4,128]{3,2,1,0:T(4,128)S(1)}, f32[4,64,4,128]{3,2,1,0:T(4,128)}, u32[]{:S(2)}) copy-start(f32[4,64,4,128]{3,2,1,0:T(4,128)} %get-tuple-element.371) | copy-start | bytes 1572868
  225.5 87.9 %copy-start.3 = (f32[4,64,4,128]{3,1,2,0:T(8,128)S(1)}, f32[4,64,4,128]{3,1,2,0:T(8,128)}, u32[]{:S(2)}) copy-start(f32[4,64,4,128]{3,1,2,0:T(8,128)} %get-tuple-element.228) | copy-start | bytes 1572868
  225.5 376.0 %all-to-all-start = ((bf16[16,512,128]{1,2,0:T(8,128)(2,1)}), bf16[16,512,128]{1,2,0:T(8,128)(2,1)}, u32[]{:S(2)}, u32[]{:S(2)}) async-start(bf16[16,512,128]{1,2,0:T(8,128)(2,1)} %stack.2), calls=%async_computation | async-start | bytes 4194304 | tf_op jit(solution)/shard_map/all_to_all | solution.py:143
  230.1 367.6 %all-gather.27.cloned.1.call-start = ((), (), s32[]{:S(2)}) async-start(), calls=%async_computation.9 | async-start | bytes 4456448 | tf_op jit(solution)/shard_map/all_gather | solution.py:145
  230.9 380.7 %reduce-scatter.2.cloned.1.call-start = ((), (), s32[]{:S(2)}) async-start(), calls=%async_computation.10 | async-start | bytes 1572864 | tf_op jit(solution)/shard_map/reduce_scatter | solution.py:216
  313.4 0.7 copy-start.8
  373.6 134.1 %copy-start.2 = (bf16[256,2048]{1,0:T(8,128)(2,1)S(1)}, bf16[256,2048]{1,0:T(8,128)(2,1)}, u32[]{:S(2)}) copy-start(bf16[256,2048]{1,0:T(8,128)(2,1)} %all-gather.13.cloned.1.call-done) | copy-start | bytes 3145732
  435.5 79.6 %copy-start.5 = (f32[128]{0:T(128)S(1)}, f32[128]{0:T(128)}, u32[]{:S(2)}) copy-start(f32[128]{0:T(128)} %param.30) | copy-start | bytes 1540
  511.6 5.2 collective-permute-start
  517.0 80.8 %copy-start.9 = (f32[1024]{0:T(1024)S(1)}, f32[1024]{0:T(1024)}, u32[]{:S(2)}) copy-start(f32[1024]{0:T(1024)} %param.35) | copy-start | bytes 12292
  517.0 80.8 %copy-start.10 = (f32[1024]{0:T(1024)S(1)}, f32[1024]{0:T(1024)}, u32[]{:S(2)}) copy-start(f32[1024]{0:T(1024)} %param.34) | copy-start | bytes 12292
Sparse Core Ops, SparseCore 0:
  8.9 11.7 all-gather.12
  23.4 61.5 all-gather.18
  87.8 59.1 all-gather.16
  149.6 59.1 all-gather.14
  211.5 78.1 all-gather.20
  292.3 61.2 all-gather.28
  356.3 74.3 all-gather.22
  433.5 74.1 all-gather.24
  510.4 87.3 all-gather.26
  605.0 6.5 reduce-scatter.1
